TPU v7x, 128 devices: a whole 4x4x4 slice. The times are simulated.
128 devices in a mesh: ep: 64 (over z, y, x), tp: 2 (over core).
Axes of the slice: x: 4, y: 4, z: 4, core: 2. Of those that a mesh axis runs over, the one named last changes fastest.
Arguments:
- tokens: bfloat16 [1024, 2048], P('ep'), may hold values from -6 to 6
- norm_attn: float32 [2048], replicated, may hold values from 0.1 to 1.9
- w_query: bfloat16 [2048, 2048], P(None, 'tp'), may hold values from -0.125 to 0.125
- w_key: bfloat16 [2048, 256], P(None, 'tp'), may hold values from -0.125 to 0.125
- w_value: bfloat16 [2048, 256], P(None, 'tp'), may hold values from -0.125 to 0.125
- w_out: bfloat16 [2048, 2048], P('tp'), may hold values from -0.125 to 0.125
- attn_bias: float32 [32], P('tp'), may hold values from -7 to -1
- cache_keys: bfloat16 [1024, 1024, 256], P('ep', None, 'tp'), may hold values from -6 to 6
- cache_values: bfloat16 [1024, 1024, 256], P('ep', None, 'tp'), may hold values from -6 to 6
- lengths: int32 [1024], P('ep'), may hold values from 256 to 1024
- norm_ffn: float32 [2048], replicated, may hold values from 0.1 to 1.9
- expert_gate: bfloat16 [2048, 57344], P(None, ('ep', 'tp')), may hold values from -0.125 to 0.125
- expert_up: bfloat16 [2048, 57344], P(None, ('ep', 'tp')), may hold values from -0.125 to 0.125
- expert_down: bfloat16 [57344, 2048], P(('ep', 'tp')), may hold values from -0.0625 to 0.0625
- dense_gate_w: bfloat16 [2048, 7168], P(None, 'ep'), may hold values from -0.125 to 0.125
- dense_up_w: bfloat16 [2048, 7168], P(None, 'ep'), may hold values from -0.125 to 0.125
- dense_down_w: bfloat16 [7168, 2048], P('ep'), may hold values from -0.0625 to 0.0625
- dense_mix: bfloat16 [2048], replicated, may hold values from -0.125 to 0.125
- routes: int32 [1024, 2], P(('ep', 'tp')), may hold values from 0 to 7, all different within a row; in each aligned block of 8 rows (0 to 7, 8 to 15, ...) at most 3 rows name the same one
- route_weights: bfloat16 [1024, 2], P(('ep', 'tp')), may hold values from 0.19921875 to 1
Outputs:
- layer_out: bfloat16 [1024, 2048], P(('ep', 'tp'))
- new_keys: bfloat16 [1024, 256], P('ep', 'tp')
- new_values: bfloat16 [1024, 256], P('ep', 'tp')
Inputs may be any that keep to these rules, and one draw needn't show every extreme that they name: `routes`: in each aligned block of 8 rows (the rows of one device) no expert is named by more than 3 rows, a bound that some block reaches; a row names 2 different experts.
All inputs are finite; a program needn't handle non-finite values.
Results may differ from a plain program's by a relative error of at most 0.015.
Values may be sent and summed in bfloat16 or wider, within the bound.
A program may use at most 128 MiB of HBM per device.

v0:
```python
import functools
import jax
import jax.numpy as jnp
from jax import lax
from jax.experimental import pallas as pl
from jax.experimental.pallas import tpu as pltpu
from jax.sharding import PartitionSpec as P

D = 2048
BF = jnp.bfloat16
F32 = jnp.float32
EPSILON = 1e-06
SEQS = 16
CACHE = 1024
HEADS = 16
NT = (((1,), (1,)), ((), ()))
VM = pl.BlockSpec(memory_space=pltpu.VMEM)
HB = pl.BlockSpec(memory_space=pltpu.HBM)


def normed_rows(widened, gain):
    scale = lax.rsqrt(jnp.mean(widened * widened, axis=-1, keepdims=True) + EPSILON)
    return (widened * scale * gain).astype(BF)


def column_of(row, count):
    rows = lax.broadcasted_iota(jnp.int32, (count, count), 0)
    cols = lax.broadcasted_iota(jnp.int32, (count, count), 1)
    wide = jnp.broadcast_to(row, (count, count))
    return jnp.sum(jnp.where(rows == cols, wide, 0.0), axis=1, keepdims=True)


HALF = D // 2
WIDE = HALF + 128
MESH = pl.DeviceIdType.MESH
GATHER = (((0, 384), (2, 1, 0)), ((384, 384), (1, 0, 2)), ((768, 384), (0, 2, 1)))
SCATTER = (((0, 384), (0, 1, 2)), ((384, 384), (2, 0, 1)), ((768, 256), (1, 2, 0)))
HIDDEN = 512
GROUP = 4
N_RECV = 102
PHASE = [None]


def phase(name):
    if PHASE[0] is not None:
        PHASE[0].__exit__(None, None, None)
    PHASE[0] = jax.named_scope(name) if name else None
    if name:
        PHASE[0].__enter__()


def layer_kernel(
    tokens, norm, bias, lengths, gain, mix_w, routes, route_w,
    wq_h, wk_h, wv_h, wo_h, ck_h, cv_h, eg_h, eu_h, ed_h, dg_h, du_h, dd_h,
    out, nk, nv,
    wq, wk, wv, wo, ckv, qs, xs, part,
    rx, mid, gath, weights, hid, ps, pin, tot, rb, fin, t1, r2, res, got,
    sq, skv, so, sw, wsem, psem, gsem, csem, rsem,
):
    phase("start")
    ep = lax.axis_index("ep")
    core = lax.axis_index("tp")
    other = 1 - core
    me = (ep // 16, lax.rem(ep // 4, 4), lax.rem(ep, 4))
    strides = (16, 4, 1)

    def shifted(axis, k):
        return lax.rem(me[axis] + (k + 4), 4)

    def chip_at(axis, k, second=0, m=0):
        far = ep + (shifted(axis, k) - me[axis]) * strides[axis]
        return far + (shifted(second, m) - me[second]) * strides[second], core

    peer = (ep, other)
    barrier = pltpu.get_barrier_semaphore()
    pl.semaphore_signal(barrier, inc=1, device_id=peer, device_id_type=MESH)
    for axis in range(3):
        for k in range(1, 4):
            pl.semaphore_signal(barrier, inc=1, device_id=chip_at(axis, k), device_id_type=MESH)
            for m in range(1, 4):
                target = chip_at(axis, k, (axis + 1) % 3, m)
                pl.semaphore_signal(barrier, inc=1, device_id=target, device_id_type=MESH)

    def q_copy(i):
        rows = pl.ds(i * 512, 512)
        return pltpu.make_async_copy(wq_h.at[rows], wq.at[rows], sq.at[i])

    def cache_start(i):
        rows = pl.ds(i * GROUP, GROUP)
        pltpu.make_async_copy(ck_h.at[rows], ckv.at[0, rows], skv.at[i]).start()
        pltpu.make_async_copy(cv_h.at[rows], ckv.at[1, rows], skv.at[i]).start()

    def cache_wait(i):
        both = ckv.at[:, pl.ds(i * GROUP, GROUP)]
        pltpu.make_async_copy(both, both, skv.at[i]).wait()

    ck, cv = ckv.at[0], ckv.at[1]
    wk_copy = pltpu.make_async_copy(wk_h, wk, sw.at[0])
    wv_copy = pltpu.make_async_copy(wv_h, wv, sw.at[1])
    for i in range(4):
        q_copy(i).start()
    cache_start(0)

    kind = lax.broadcasted_iota(jnp.int32, (8, 128), 1)
    meta = jnp.zeros((8, 128), F32)
    for k in range(2):
        chosen = column_of(routes[k : k + 1, :].astype(F32), 8).astype(jnp.int32)
        share = column_of(route_w[k : k + 1, :].astype(F32), 8)
        meta += jnp.where(kind == chosen, share, 0.0)
    part[core, :, D : D + 128] = meta.astype(BF)
    part[other, :, D : D + 128] = jnp.zeros((8, 128), BF)

    normed_all = normed_rows(jnp.concatenate([tokens[0].astype(F32), tokens[1].astype(F32)], axis=0), norm[...])
    phase("query")
    query = jnp.zeros((SEQS, HEADS * 64), F32)
    for i in range(4):
        q_copy(i).wait()
        if i < 3:
            cache_start(i + 1)
        query += jnp.dot(normed_all[:, i * 512 : (i + 1) * 512], wq[pl.ds(i * 512, 512), :], preferred_element_type=F32)
    for i in range(16):
        row = (i % 8) * 128 + (i // 8) * 64
        pltpu.make_async_copy(wo_h.at[pl.ds(i * 64, 64)], wo.at[pl.ds(row, 64)], so).start()
    wk_copy.start()
    wv_copy.start()
    query = query.astype(BF).astype(F32) * 0.125
    lane = lax.broadcasted_iota(jnp.int32, (SEQS, 128), 1)
    for i in range(8):
        pair = query[:, i * 128 : (i + 1) * 128]
        turned = pltpu.roll(pair, 64, 1)
        for j in range(2):
            h = 2 * i + j
            low = h < 8
            chosen = pair if (j == 0) == low else turned
            keep = (lane < 64) if low else (lane >= 64)
            qs[:, h, :] = jnp.where(keep, chosen, 0.0)

    phase("attend")
    bias_col = column_of(bias[...], HEADS)
    tri = (
        lax.broadcasted_iota(jnp.int32, (256, 256), 0) > lax.broadcasted_iota(jnp.int32, (256, 256), 1)
    ).astype(BF)
    places = lax.broadcasted_iota(jnp.int32, (HEADS, CACHE), 1)
    lane8 = lax.broadcasted_iota(jnp.int32, (8, 128), 1)

    def some(i, carry):
        group = [i * GROUP + j for j in range(GROUP)]
        cache_wait(i)
        scores = [
            lax.dot_general(qs[b].astype(BF), ck[b], NT, preferred_element_type=F32) + bias_col for b in group
        ]
        takes, keeps, seen, stacked = [], [], [], []
        for b, z in zip(group, scores):
            visible = places < lengths[b]
            tail = jnp.log(1.0 + jnp.exp(-jnp.abs(z)))
            log_take = jnp.minimum(z, 0.0) - tail
            log_keep = jnp.where(visible, log_take - z, 0.0)
            high = log_keep.astype(BF)
            rest = (log_keep - high.astype(F32)).astype(BF)
            takes.append(log_take)
            keeps.append(log_keep)
            seen.append(visible)
            for n in range(4):
                stacked.append(high[:, n * 256 : (n + 1) * 256])
                stacked.append(rest[:, n * 256 : (n + 1) * 256])
        sums = jnp.dot(jnp.concatenate(stacked, axis=0), tri, preferred_element_type=F32)
        weights = []
        for at in range(GROUP):
            later = jnp.zeros((HEADS, 1), F32)
            after = [None] * 4
            for n in range(3, -1, -1):
                row = at * 128 + n * 32
                inner = sums[row : row + 16] + sums[row + 16 : row + 32]
                after[n] = inner + later
                later = later + inner[:, 0:1] + keeps[at][:, n * 256 : n * 256 + 1]
            after = jnp.concatenate(after, axis=1)
            weights.append(jnp.where(seen[at], jnp.exp(takes[at] + after), 0.0).astype(BF))
        for b, weight in zip(group, weights):
            mixed = jnp.dot(weight, cv[b], preferred_element_type=F32)
            xs[b] = jnp.where(lane8 < 64, mixed[0:8], mixed[8:16])
        return carry

    lax.fori_loop(0, SEQS // GROUP, some, 0)

    phase("project")
    base = pl.multiple_of(core * 48, 16)
    loads = (
        (eg_h, 0, 448), (dg_h.at[pl.ds(base, 64)], 448, 64),
        (eu_h, 512, 448), (du_h.at[pl.ds(base, 64)], 960, 64),
        (ed_h, 1024, 448), (dd_h.at[pl.ds(base, 64)], 1472, 64),
    )
    for src, row, count in loads:
        pltpu.make_async_copy(src, weights.at[pl.ds(row, count)], wsem).start()
    pltpu.make_async_copy(wo, wo, so).wait()
    heads = jnp.concatenate([xs[:, r, :].astype(BF) for r in range(8)], axis=1)
    value = jnp.dot(heads, wo[...], preferred_element_type=F32)
    part[0, :, 0:D] = value[0:8].astype(BF)
    part[1, :, 0:D] = value[8:16].astype(BF)

    used = [0]

    def slots(count):
        used[0] += count
        return list(range(used[0] - count, used[0]))

    def send(src, dst, device, sem, slot):
        pltpu.make_async_remote_copy(
            src_ref=src, dst_ref=dst, send_sem=sem, recv_sem=rsem.at[slot], device_id=device, device_id_type=MESH
        ).start()

    def arrived(ref, slot):
        pltpu.make_async_remote_copy(
            src_ref=ref, dst_ref=ref, send_sem=csem, recv_sem=rsem.at[slot], device_id=peer, device_id_type=MESH
        ).wait_recv()

    pl.semaphore_wait(barrier, 37)
    phase("pair")
    (slot,) = slots(1)
    send(part, rx, peer, psem, slot)
    wk_copy.wait()
    wv_copy.wait()
    nk[...] = jnp.dot(normed_all, wk[...], preferred_element_type=F32).astype(BF)
    nv[...] = jnp.dot(normed_all, wv[...], preferred_element_type=F32).astype(BF)
    arrived(rx, slot)
    phase("norm")
    mix_row = mix_w[...].astype(F32).reshape(1, D)
    for h in range(2):
        summed = part[h].astype(F32) + rx[h].astype(F32)
        middle = (tokens[h].astype(F32) + summed[:, 0:D]).astype(BF).astype(F32)
        normed = normed_rows(middle, gain[...]).astype(F32)
        mix = jax.nn.sigmoid(jnp.sum(normed * mix_row, axis=1, keepdims=True))
        mix_high = mix.astype(BF).astype(F32)
        meta = jnp.where(kind == 8, mix_high, summed[:, D : D + 128])
        meta = jnp.where(kind == 9, mix - mix_high, meta)
        mid[h] = jnp.where(core == 0, middle[:, 0:HALF], middle[:, HALF:D])
        own = jnp.where(core == 0, normed[:, 0:HALF], normed[:, HALF:D])
        gath[h, core, me[0], me[1], me[2], :, 0:HALF] = own.astype(BF)
        gath[h, core, me[0], me[1], me[2], :, HALF:WIDE] = meta.astype(BF)

    whole = pl.ds(0, 4)
    parts = range(3)
    steps = (1, -1, 2)
    upward, downward = (0, 2), (1, -1)
    g2 = gath.reshape(2, 2, 512, WIDE)

    def sized(rows, lanes):
        return g2.at[0, 0, pl.ds(0, rows), pl.ds(lanes[0], lanes[1])]

    class Gather:
        def __init__(self, h):
            self.h = h
            self.first = slots(3)
            self.second = [dict(zip(steps, slots(3))) for p in parts]
            self.below = [dict(zip((0, 2, 1), slots(3))) for p in parts]
            self.above = [dict(zip((1, -1, 0), slots(3))) for p in parts]
            for p in parts:
                self.below[p][-1] = self.below[p][1]
                self.above[p][2] = self.above[p][0]
            self.relayed = slots(3)
            (self.across,) = slots(1)

        def held(self, lanes, where):
            at = [me[0], me[1], me[2]]
            for axis, index in where.items():
                at[axis] = index
            return gath.at[self.h, core, at[0], at[1], at[2], :, pl.ds(lanes[0], lanes[1])]

        def spread(self, block, device, slot):
            send(block, block, device, gsem, slot)

        def plane(self):
            for m in (0, *steps):
                for k in (0, *steps):
                    for p, (lanes, (a, b, c)) in enumerate(GATHER):
                        if (k, m) != (0, 0):
                            slot = self.second[p][m] if m else self.first[p]
                            self.spread(self.held(lanes, {}), chip_at(a, k, b, m), slot)

        def bulk(self, p, o):
            lanes, (a, b, c) = GATHER[p]
            if o:
                arrived(sized(32, lanes), self.second[p][-o if o != 2 else 2])
            else:
                arrived(sized(24, lanes), self.first[p])
            block = self.held(lanes, {a: whole, b: shifted(b, o)})
            self.spread(block, chip_at(c, 1), self.below[p][o])
            self.spread(block, chip_at(c, -1), self.above[p][o])

        def rounds(self):
            for o in (0, *steps):
                for p in parts:
                    self.bulk(p, o)
            for p in parts:
                self.hand_over(p, 0)

        def hand_over(self, p, o):
            lanes, (a, b, c) = GATHER[p]
            self.spread(self.held(lanes, {a: whole, b: whole, c: shifted(c, o)}), peer, self.across)

        def relay(self, o):
            for p, (lanes, (a, b, c)) in enumerate(GATHER):
                below = o in upward
                arrived(sized(32, lanes), (self.below if below else self.above)[p][o])
                block = self.held(lanes, {a: whole, b: shifted(b, o), c: shifted(c, -1 if below else 1)})
                self.spread(block, chip_at(c, 1 if below else -1), self.relayed[p])

        def neighbours(self):
            for p, (lanes, _) in enumerate(GATHER):
                arrived(sized(64, lanes), self.below[p][1])
                self.hand_over(p, -1)
                arrived(sized(64, lanes), self.above[p][0])
                self.hand_over(p, 1)

        def farthest(self):
            for p, (lanes, _) in enumerate(GATHER):
                arrived(sized(128, lanes), self.relayed[p])
                self.hand_over(p, 2)

        def complete(self):
            arrived(g2.at[self.h, 0], self.across)

    expert = ep // 8
    column = lax.broadcasted_iota(jnp.int32, (1, 256), 1) + 256
    dense_own = jnp.logical_and(column >= 448, jnp.logical_or(core == 0, column >= 464))
    kinds = lax.broadcasted_iota(jnp.int32, (256, 128), 1)

    def hidden_unit(h, i, n):
        rows = slice(i * 256, (i + 1) * 256)
        x = [g2[h, c, rows, 0:HALF] for c in range(2)]
        info = g2[h, 0, rows, HALF:WIDE].astype(F32)
        factor = jnp.sum(jnp.where(kinds == expert, info, 0.0), axis=1, keepdims=True)
        if n == 1:
            mixed = info[:, 8:9] + info[:, 9:10]
            factor = jnp.where(column < 448, factor, jnp.where(dense_own, mixed, 0.0))

        def product(row):
            w = weights[row : row + 256, :]
            y = lax.dot_general(x[0], w[:, 0:HALF], NT, preferred_element_type=F32)
            return y + lax.dot_general(x[1], w[:, HALF:D], NT, preferred_element_type=F32)

        g = product(n * 256)
        u = product(HIDDEN + n * 256)
        hid[h, rows, n * 256 : (n + 1) * 256] = g * jax.nn.sigmoid(g) * u * factor

    h4 = hid.reshape(2, 4, 4, 4, 8, HIDDEN)
    halves = (pl.ds(0, 2), pl.ds(2, 2))

    def place(axis, index):
        at = [slice(None)] * 3
        at[axis] = index
        return tuple(at)

    def summand(ref, lanes, axis, where, half=None):
        at = [whole, whole, whole]
        at[axis] = where
        if half is not None:
            at[1 if axis == 0 else 0] = half
        return ref.at[at[0], at[1], at[2], :, pl.ds(lanes[0], lanes[1])]

    def cells(axis, index):
        for i in range(4):
            for j in range(4):
                at = [i, j]
                at.insert(axis, index)
                yield i, j, tuple(at)

    offsets = [(m, k) for m in (2, 1, -1, 0) for k in (2, 1, -1, 0) if (m, k) != (0, 0)]

    class Scatter:
        def __init__(self, h):
            self.h = h
            self.swap = dict(zip((2, 1, -1, 0), slots(4)))
            self.far = [slots(2) for p in parts]
            self.last = slots(3)
            self.nexts = slots(3)

        def down(self, o):
            h = self.h
            for p, (lanes, (a, b, c)) in enumerate(SCATTER):
                cut = slice(lanes[0], lanes[0] + lanes[1])
                high = slice(HALF + lanes[0], HALF + lanes[0] + lanes[1])
                rows = place(a, shifted(a, o))
                x = h4[(h,) + rows + (slice(None), slice(None))].reshape(128, HIDDEN).astype(BF)
                w = jnp.concatenate([weights[2 * HIDDEN :, cut], weights[2 * HIDDEN :, high]], axis=1)
                y = jnp.dot(x, w, preferred_element_type=F32)
                for half in range(2):
                    piece = y[:, half * lanes[1] : (half + 1) * lanes[1]].reshape(4, 4, 8, lanes[1])
                    ps[(h, half) + rows + (slice(None), cut)] = piece.astype(BF)
                send(
                    summand(ps.at[h, other], lanes, a, shifted(a, o)), summand(pin.at[h], lanes, a, shifted(a, o)),
                    peer, csem, self.swap[o],
                )

        def joined(self, p, o):
            h = self.h
            lanes, (a, b, c) = SCATTER[p]
            cut = slice(lanes[0], lanes[0] + lanes[1])
            if p == 0:
                arrived(pin.at[h, 0], self.swap[o])
            for i, j, at in cells(a, shifted(a, o)):
                at = at + (slice(None), cut)
                tot[(h,) + at] = (ps[(h, core) + at].astype(F32) + pin[(h,) + at].astype(F32)).astype(BF)

        def open(self):
            h = self.h
            for p, (lanes, (a, b, c)) in enumerate(SCATTER):
                self.joined(p, 2)
                for way, k in enumerate((1, -1)):
                    send(
                        summand(tot.at[h], lanes, a, shifted(a, 2), halves[way]),
                        rb.at[h, way, :, :, :, pl.ds(lanes[0], lanes[1])],
                        chip_at(a, k), csem, self.far[p][way],
                    )

        def near(self, k):
            h = self.h
            way = 0 if k == 1 else 1
            half = halves[1 - way]
            for p, (lanes, (a, b, c)) in enumerate(SCATTER):
                self.joined(p, k)
                send(
                    summand(tot.at[h], lanes, a, shifted(a, k), half),
                    fin.at[h, way, half, :, :, pl.ds(lanes[0], lanes[1])],
                    chip_at(a, k), csem, self.last[p],
                )

        def close(self):
            h = self.h
            for p, (lanes, (a, b, c)) in enumerate(SCATTER):
                cut = slice(lanes[0], lanes[0] + lanes[1])
                lanes_ds = pl.ds(lanes[0], lanes[1])
                for way, k in enumerate((1, -1)):
                    arrived(rb.at[h, way, :, :, :, lanes_ds], self.far[p][way])
                    for i, j, at in cells(a, shifted(a, k)):
                        if i // 2 == way:
                            at = (h,) + at + (slice(None), cut)
                            tot[at] = (tot[at].astype(F32) + rb[h, way, i % 2, j, :, cut].astype(F32)).astype(BF)
                    send(
                        summand(tot.at[h], lanes, a, shifted(a, k), halves[way]),
                        fin.at[h, way, halves[way], :, :, lanes_ds],
                        chip_at(a, k), csem, self.last[p],
                    )

        def own(self):
            for p in parts:
                self.joined(p, 0)

        def plane(self):
            h = self.h
            for p, (lanes, (a, b, c)) in enumerate(SCATTER):
                cut = slice(lanes[0], lanes[0] + lanes[1])
                lanes_ds = pl.ds(lanes[0], lanes[1])
                arrived(fin.at[h, :, :, :, :, lanes_ds], self.last[p])
                for i, j, at in cells(a, me[a]):
                    t1[h, i, j, :, cut] = (
                        tot[(h,) + at + (slice(None), cut)].astype(F32)
                        + fin[h, 0, i, j, :, cut].astype(F32)
                        + fin[h, 1, i, j, :, cut].astype(F32)
                    ).astype(BF)
                d, e = [axis for axis in range(3) if axis != a]
                for n, (m, k) in enumerate(offsets):
                    send(
                        t1.at[h, shifted(d, m), shifted(e, k), :, lanes_ds], r2.at[h, n, :, lanes_ds],
                        chip_at(d, m, e, k), csem, self.nexts[p],
                    )

        def total(self):
            h = self.h
            for p, (lanes, (a, b, c)) in enumerate(SCATTER):
                cut = slice(lanes[0], lanes[0] + lanes[1])
                arrived(r2.at[h, :, :, pl.ds(lanes[0], lanes[1])], self.nexts[p])
                d, e = [axis for axis in range(3) if axis != a]
                sum_ = mid[h, :, cut] + t1[h, me[d], me[e], :, cut].astype(F32)
                for n in range(15):
                    sum_ += r2[h, n, :, cut].astype(F32)
                res[h, :, cut] = sum_.astype(BF)

    phase("gather1")
    ga, gb = Gather(0), Gather(1)
    sa, sb = Scatter(0), Scatter(1)
    ga.plane()
    gb.plane()
    phase("gather2")
    ga.rounds()
    phase("gather3")
    ga.relay(0)
    gb.rounds()
    phase("gather4")
    for o in steps:
        ga.relay(o)
    gb.relay(0)
    ga.neighbours()
    phase("gather5")
    for o in steps:
        gb.relay(o)
    ga.farthest()
    pltpu.make_async_copy(weights, weights, wsem).wait()
    ga.complete()
    phase("hidden_a")
    hidden_unit(0, 0, 0)
    hidden_unit(0, 0, 1)
    gb.neighbours()
    hidden_unit(0, 1, 0)
    hidden_unit(0, 1, 1)
    phase("down_a")
    sa.down(2)
    gb.farthest()
    sa.down(1)
    sa.open()
    sa.down(-1)
    sa.near(1)
    sa.down(0)
    sa.near(-1)
    phase("complete_b")
    gb.complete()
    phase("hidden_b")
    hidden_unit(1, 0, 0)
    sa.own()
    hidden_unit(1, 0, 1)
    sa.close()
    hidden_unit(1, 1, 0)
    hidden_unit(1, 1, 1)
    phase("down_b")
    sb.down(2)
    sb.down(1)
    sb.open()
    phase("plane_a")
    sa.plane()
    phase("near_b")
    sb.down(-1)
    sb.near(1)
    sb.down(0)
    sb.near(-1)
    phase("close_b")
    sb.close()
    sb.own()
    phase("total_a")
    sa.total()
    phase("plane_b")
    sb.plane()
    phase("total_b")
    sb.total()
    phase("exchange")
    (slot,) = slots(1)
    send(res.at[other], got, peer, csem, slot)
    out[core] = res[core]
    arrived(got, slot)
    out[other] = got[...]
    phase("finish")
    assert used[0] == N_RECV, used[0]
    rows = gath.reshape(2048, WIDE).at[pl.ds(0, 2032)]
    pltpu.make_async_copy(rows, rows, gsem).wait()
    rows = ps.reshape(2048, HALF).at[pl.ds(0, 2040)]
    pltpu.make_async_copy(rows, rows, csem).wait()
    pltpu.make_async_copy(part, part, psem).wait()
    phase(None)


def finish_kernel(a, b, c, out, nk, nv):
    out[:, 0:HALF] = a[0]
    out[:, HALF:D] = a[1]
    nk[...] = b[...]
    nv[...] = c[...]


OUT_SHAPES = (
    jax.ShapeDtypeStruct((8, D), BF),
    jax.ShapeDtypeStruct((SEQS, 128), BF),
    jax.ShapeDtypeStruct((SEQS, 128), BF),
)


def layer(*args):
    return pl.pallas_call(
        layer_kernel,
        out_shape=(jax.ShapeDtypeStruct((2, 8, HALF), BF),) + OUT_SHAPES[1:],
        in_specs=[VM] * 3 + [pl.BlockSpec(memory_space=pltpu.SMEM)] + [VM] * 4 + [HB] * 12,
        out_specs=(VM, VM, VM),
        scratch_shapes=[
            pltpu.VMEM((D, 1024), BF),
            pltpu.VMEM((D, 128), BF),
            pltpu.VMEM((D, 128), BF),
            pltpu.VMEM((1024, D), BF),
            pltpu.VMEM((2, SEQS, CACHE, 128), BF),
            pltpu.VMEM((SEQS, HEADS, 128), F32),
            pltpu.VMEM((SEQS, 8, 128), F32),
            pltpu.VMEM((2, 8, D + 128), BF),
            pltpu.VMEM((2, 8, D + 128), BF),
            pltpu.VMEM((2, 8, HALF), F32),
            pltpu.VMEM((2, 2, 4, 4, 4, 8, WIDE), BF),
            pltpu.VMEM((3 * HIDDEN, D), BF),
            pltpu.VMEM((2, 512, HIDDEN), F32),
            pltpu.VMEM((2, 2, 4, 4, 4, 8, HALF), BF),
            pltpu.VMEM((2, 4, 4, 4, 8, HALF), BF),
            pltpu.VMEM((2, 4, 4, 4, 8, HALF), BF),
            pltpu.VMEM((2, 2, 2, 4, 8, HALF), BF),
            pltpu.VMEM((2, 2, 4, 4, 8, HALF), BF),
            pltpu.VMEM((2, 4, 4, 8, HALF), BF),
            pltpu.VMEM((2, 15, 8, HALF), BF),
            pltpu.VMEM((2, 8, HALF), BF),
            pltpu.VMEM((8, HALF), BF),
            pltpu.SemaphoreType.DMA((4,)),
            pltpu.SemaphoreType.DMA((4,)),
            pltpu.SemaphoreType.DMA,
            pltpu.SemaphoreType.DMA((2,)),
            pltpu.SemaphoreType.DMA,
            pltpu.SemaphoreType.DMA,
            pltpu.SemaphoreType.DMA,
            pltpu.SemaphoreType.DMA,
            pltpu.SemaphoreType.DMA((N_RECV,)),
        ],
        compiler_params=pltpu.CompilerParams(
            vmem_limit_bytes=63 * 1024 * 1024, collective_id=0, has_side_effects=True
        ),
        name="layer",
    )(*args)


def shards(
    tokens, norm_attn, w_query, w_key, w_value, w_out, attn_bias, cache_keys, cache_values, lengths,
    norm_ffn, expert_gate, expert_up, expert_down, dense_gate_w, dense_up_w, dense_down_w, dense_mix,
    routes, route_weights,
):
    results = layer(
        tokens.reshape(2, 8, D), norm_attn.reshape(1, D), attn_bias.reshape(1, HEADS), lengths,
        norm_ffn.reshape(1, D), dense_mix, routes.T, route_weights.T,
        w_query, w_key, w_value, w_out, cache_keys, cache_values,
        expert_gate.T, expert_up.T, expert_down, dense_gate_w.T, dense_up_w.T, dense_down_w,
    )
    return pl.pallas_call(
        finish_kernel, out_shape=OUT_SHAPES, in_specs=[VM] * 3, out_specs=(VM, VM, VM), name="finish"
    )(*results)


def solution(mesh):
    placed = (
        P("ep", None),
        P(),
        P(None, "tp"),
        P(None, "tp"),
        P(None, "tp"),
        P("tp", None),
        P("tp"),
        P("ep", None, "tp"),
        P("ep", None, "tp"),
        P("ep"),
        P(),
        P(None, ("ep", "tp")),
        P(None, ("ep", "tp")),
        P(("ep", "tp"), None),
        P(None, "ep"),
        P(None, "ep"),
        P("ep", None),
        P(),
        P(("ep", "tp"), None),
        P(("ep", "tp"), None),
    )
    return jax.shard_map(
        shards,
        mesh=mesh,
        in_specs=placed,
        out_specs=(P(("ep", "tp"), None), P("ep", "tp"), P("ep", "tp")),
        check_vma=False,
    )
```

profile of v0, /device:TPU:1, one launch (start us, length us, event | category | flops | bytes accessed | tf_op | source)
XLA Modules:
  0.0 60.1 jit_solution(1150088949353017544)
XLA Ops:
  0.6 58.0 %layer.1 = (bf16[2,8,1024]{2,1,0:T(8,128)(2,1)}, bf16[16,128]{1,0:T(8,128)(2,1)}, bf16[16,128]{1,0:T(8,128)(2,1)}) custom-call(bf16[2,8,2048]{2,1,0:T(8,128)(2,1)} %bitcast.14, f32[1,2048]{1,0:T(1,128)} %bitcast.15, f32[1,16]{1,0:T(1,128)} %bitcast.18, s32[16]{0:T(128)} %lengths.1, f32[1,2048]{1,0:T(1,128)} %bitcast.16, bf16[2048]{0:T(1024)(128)(2,1)} %mix_w.1, ...), custom_call_target="tpu_custom_call" | custom-call | tf_op jit(solution)/shard_map/layer/pallas_call | solution.py:574
  58.7 1.4 %finish.1 = (bf16[8,2048]{1,0:T(8,128)(2,1)}, bf16[16,128]{1,0:T(8,128)(2,1)}, bf16[16,128]{1,0:T(8,128)(2,1)}) custom-call(bf16[2,8,1024]{2,1,0:T(8,128)(2,1)} %get-tuple-element.6.a, bf16[16,128]{1,0:T(8,128)(2,1)} %get-tuple-element.7.b, bf16[16,128]{1,0:T(8,128)(2,1)} %get-tuple-element.8.c), custom_call_target="tpu_custom_call" | custom-call | tf_op jit(solution)/shard_map/finish/pallas_call | solution.py:630
where the time goes:
time: 60.3 us; the launch traced here: 60.1 us
  Pallas kernels  59.4 us (99%)
  between operations  0.65 us (1%)
    pallas_call x1, Pallas kernels, layer(): pl.pallas_call(layer_kernel, out_shape=(jax.ShapeDtypeStruct((2, 8, HALF)...  58 us
    pallas_call x1, Pallas kernels, shards(): pl.pallas_call(finish_kernel, out_shape=OUT_SHAPES, in_specs=[VM] * 3, ou...  1.39 us

commit v1 on v0

--- a/solution.py
+++ b/solution.py
@@ -37,7 +37,8 @@
 SCATTER = (((0, 384), (0, 1, 2)), ((384, 384), (2, 0, 1)), ((768, 256), (1, 2, 0)))
 HIDDEN = 512
 GROUP = 4
-N_RECV = 102
+DIRECT = (True, True, True, True)
+N_RECV = 99 - 12 * sum(DIRECT[0:2]) - 6 * sum(DIRECT[2:4])
 PHASE = [None]
 
 
@@ -50,11 +51,12 @@
 
 
 def layer_kernel(
-    tokens, norm, bias, lengths, gain, mix_w, routes, route_w,
+    tokens_h, norm_h, bias_h, lengths_h, gain_h, mix_h, routes_h, route_w_h,
     wq_h, wk_h, wv_h, wo_h, ck_h, cv_h, eg_h, eu_h, ed_h, dg_h, du_h, dd_h,
     out, nk, nv,
+    tokens, norm, bias, lengths, gain, mix_w, routes, route_w, small,
     wq, wk, wv, wo, ckv, qs, xs, part,
-    rx, mid, gath, weights, hid, ps, pin, tot, rb, fin, t1, r2, res, got,
+    rx, mid, gath, weights, hid, ps, own_sum, pin, tot, rb, fin, t1, r2, res, got,
     sq, skv, so, sw, wsem, psem, gsem, csem, rsem,
 ):
     phase("start")
@@ -71,6 +73,41 @@
         far = ep + (shifted(axis, k) - me[axis]) * strides[axis]
         return far + (shifted(second, m) - me[second]) * strides[second], core
 
+    def q_copy(i):
+        rows = pl.ds(i * 512, 512)
+        return pltpu.make_async_copy(wq_h.at[rows], wq.at[rows], sq.at[i])
+
+    def cache_start(i):
+        rows = pl.ds(i * GROUP, GROUP)
+        pltpu.make_async_copy(ck_h.at[rows], ckv.at[0, rows], skv.at[i]).start()
+        pltpu.make_async_copy(cv_h.at[rows], ckv.at[1, rows], skv.at[i]).start()
+
+    def cache_wait(i):
+        both = ckv.at[:, pl.ds(i * GROUP, GROUP)]
+        pltpu.make_async_copy(both, both, skv.at[i]).wait()
+
+    ck, cv = ckv.at[0], ckv.at[1]
+    wk_copy = pltpu.make_async_copy(wk_h, wk, sw.at[0])
+    wv_copy = pltpu.make_async_copy(wv_h, wv, sw.at[1])
+    def output_start():
+        for i in range(16):
+            row = (i % 8) * 128 + (i // 8) * 64
+            pltpu.make_async_copy(wo_h.at[pl.ds(i * 64, 64)], wo.at[pl.ds(row, 64)], so).start()
+
+    littles = [
+        pltpu.make_async_copy(src, dst, small.at[n])
+        for n, (src, dst) in enumerate((
+            (tokens_h, tokens), (norm_h, norm), (routes_h, routes), (route_w_h, route_w),
+            (bias_h, bias), (lengths_h, lengths), (gain_h, gain), (mix_h, mix_w),
+        ))
+    ]
+    for copy in littles[:4]:
+        copy.start()
+    for i in range(4):
+        q_copy(i).start()
+    for copy in littles[4:]:
+        copy.start()
+    cache_start(0)
     peer = (ep, other)
     barrier = pltpu.get_barrier_semaphore()
     pl.semaphore_signal(barrier, inc=1, device_id=peer, device_id_type=MESH)
@@ -81,25 +118,8 @@
                 target = chip_at(axis, k, (axis + 1) % 3, m)
                 pl.semaphore_signal(barrier, inc=1, device_id=target, device_id_type=MESH)
 
-    def q_copy(i):
-        rows = pl.ds(i * 512, 512)
-        return pltpu.make_async_copy(wq_h.at[rows], wq.at[rows], sq.at[i])
-
-    def cache_start(i):
-        rows = pl.ds(i * GROUP, GROUP)
-        pltpu.make_async_copy(ck_h.at[rows], ckv.at[0, rows], skv.at[i]).start()
-        pltpu.make_async_copy(cv_h.at[rows], ckv.at[1, rows], skv.at[i]).start()
-
-    def cache_wait(i):
-        both = ckv.at[:, pl.ds(i * GROUP, GROUP)]
-        pltpu.make_async_copy(both, both, skv.at[i]).wait()
-
-    ck, cv = ckv.at[0], ckv.at[1]
-    wk_copy = pltpu.make_async_copy(wk_h, wk, sw.at[0])
-    wv_copy = pltpu.make_async_copy(wv_h, wv, sw.at[1])
-    for i in range(4):
-        q_copy(i).start()
-    cache_start(0)
+    for copy in littles[:4]:
+        copy.wait()
 
     kind = lax.broadcasted_iota(jnp.int32, (8, 128), 1)
     meta = jnp.zeros((8, 128), F32)
@@ -115,12 +135,11 @@
     query = jnp.zeros((SEQS, HEADS * 64), F32)
     for i in range(4):
         q_copy(i).wait()
-        if i < 3:
-            cache_start(i + 1)
+        if i == 1:
+            output_start()
+        else:
+            cache_start((1, 0, 2, 3)[i])
         query += jnp.dot(normed_all[:, i * 512 : (i + 1) * 512], wq[pl.ds(i * 512, 512), :], preferred_element_type=F32)
-    for i in range(16):
-        row = (i % 8) * 128 + (i // 8) * 64
-        pltpu.make_async_copy(wo_h.at[pl.ds(i * 64, 64)], wo.at[pl.ds(row, 64)], so).start()
     wk_copy.start()
     wv_copy.start()
     query = query.astype(BF).astype(F32) * 0.125
@@ -136,6 +155,8 @@
             qs[:, h, :] = jnp.where(keep, chosen, 0.0)
 
     phase("attend")
+    for copy in littles[4:]:
+        copy.wait()
     bias_col = column_of(bias[...], HEADS)
     tri = (
         lax.broadcasted_iota(jnp.int32, (256, 256), 0) > lax.broadcasted_iota(jnp.int32, (256, 256), 1)
@@ -143,7 +164,7 @@
     places = lax.broadcasted_iota(jnp.int32, (HEADS, CACHE), 1)
     lane8 = lax.broadcasted_iota(jnp.int32, (8, 128), 1)
 
-    def some(i, carry):
+    def attend(i):
         group = [i * GROUP + j for j in range(GROUP)]
         cache_wait(i)
         scores = [
@@ -178,24 +199,10 @@
         for b, weight in zip(group, weights):
             mixed = jnp.dot(weight, cv[b], preferred_element_type=F32)
             xs[b] = jnp.where(lane8 < 64, mixed[0:8], mixed[8:16])
-        return carry
-
-    lax.fori_loop(0, SEQS // GROUP, some, 0)
-
-    phase("project")
-    base = pl.multiple_of(core * 48, 16)
-    loads = (
-        (eg_h, 0, 448), (dg_h.at[pl.ds(base, 64)], 448, 64),
-        (eu_h, 512, 448), (du_h.at[pl.ds(base, 64)], 960, 64),
-        (ed_h, 1024, 448), (dd_h.at[pl.ds(base, 64)], 1472, 64),
-    )
-    for src, row, count in loads:
-        pltpu.make_async_copy(src, weights.at[pl.ds(row, count)], wsem).start()
-    pltpu.make_async_copy(wo, wo, so).wait()
-    heads = jnp.concatenate([xs[:, r, :].astype(BF) for r in range(8)], axis=1)
-    value = jnp.dot(heads, wo[...], preferred_element_type=F32)
-    part[0, :, 0:D] = value[0:8].astype(BF)
-    part[1, :, 0:D] = value[8:16].astype(BF)
+
+    def project(h):
+        heads = jnp.concatenate([xs[h * 8 : (h + 1) * 8, r, :].astype(BF) for r in range(8)], axis=1)
+        part[h, :, 0:D] = jnp.dot(heads, wo[...], preferred_element_type=F32).astype(BF)
 
     used = [0]
 
@@ -213,18 +220,14 @@
             src_ref=ref, dst_ref=ref, send_sem=csem, recv_sem=rsem.at[slot], device_id=peer, device_id_type=MESH
         ).wait_recv()
 
-    pl.semaphore_wait(barrier, 37)
-    phase("pair")
-    (slot,) = slots(1)
-    send(part, rx, peer, psem, slot)
-    wk_copy.wait()
-    wv_copy.wait()
-    nk[...] = jnp.dot(normed_all, wk[...], preferred_element_type=F32).astype(BF)
-    nv[...] = jnp.dot(normed_all, wv[...], preferred_element_type=F32).astype(BF)
-    arrived(rx, slot)
-    phase("norm")
+    pair_slots = slots(2)
     mix_row = mix_w[...].astype(F32).reshape(1, D)
-    for h in range(2):
+
+    def pair(h):
+        send(part.at[h], rx.at[h], peer, psem, pair_slots[h])
+
+    def norm_half(h):
+        arrived(rx.at[h], pair_slots[h])
         summed = part[h].astype(F32) + rx[h].astype(F32)
         middle = (tokens[h].astype(F32) + summed[:, 0:D]).astype(BF).astype(F32)
         normed = normed_rows(middle, gain[...]).astype(F32)
@@ -247,17 +250,20 @@
         return g2.at[0, 0, pl.ds(0, rows), pl.ds(lanes[0], lanes[1])]
 
     class Gather:
-        def __init__(self, h):
-            self.h = h
+        def __init__(self, h, direct):
+            self.h, self.direct = h, direct
             self.first = slots(3)
             self.second = [dict(zip(steps, slots(3))) for p in parts]
+            (self.across,) = slots(1)
+            if direct:
+                self.straight = [dict(zip(steps, slots(3))) for p in parts]
+                return
             self.below = [dict(zip((0, 2, 1), slots(3))) for p in parts]
             self.above = [dict(zip((1, -1, 0), slots(3))) for p in parts]
             for p in parts:
                 self.below[p][-1] = self.below[p][1]
                 self.above[p][2] = self.above[p][0]
             self.relayed = slots(3)
-            (self.across,) = slots(1)
 
         def held(self, lanes, where):
             at = [me[0], me[1], me[2]]
@@ -283,6 +289,10 @@
             else:
                 arrived(sized(24, lanes), self.first[p])
             block = self.held(lanes, {a: whole, b: shifted(b, o)})
+            if self.direct:
+                for k in (2, 1, -1):
+                    self.spread(block, chip_at(c, k), self.straight[p][k])
+                return
             self.spread(block, chip_at(c, 1), self.below[p][o])
             self.spread(block, chip_at(c, -1), self.above[p][o])
 
@@ -305,6 +315,12 @@
                 self.spread(block, chip_at(c, 1 if below else -1), self.relayed[p])
 
         def neighbours(self):
+            if self.direct:
+                for p, (lanes, _) in enumerate(GATHER):
+                    for k in (1, -1):
+                        arrived(sized(128, lanes), self.straight[p][k])
+                        self.hand_over(p, -k)
+                return
             for p, (lanes, _) in enumerate(GATHER):
                 arrived(sized(64, lanes), self.below[p][1])
                 self.hand_over(p, -1)
@@ -313,7 +329,7 @@
 
         def farthest(self):
             for p, (lanes, _) in enumerate(GATHER):
-                arrived(sized(128, lanes), self.relayed[p])
+                arrived(sized(128, lanes), self.straight[p][2] if self.direct else self.relayed[p])
                 self.hand_over(p, 2)
 
         def complete(self):
@@ -340,15 +356,9 @@
 
         g = product(n * 256)
         u = product(HIDDEN + n * 256)
-        hid[h, rows, n * 256 : (n + 1) * 256] = g * jax.nn.sigmoid(g) * u * factor
-
-    h4 = hid.reshape(2, 4, 4, 4, 8, HIDDEN)
+        hid[h, rows, n * 256 : (n + 1) * 256] = (g * jax.nn.sigmoid(g) * u * factor).astype(BF)
+
     halves = (pl.ds(0, 2), pl.ds(2, 2))
-
-    def place(axis, index):
-        at = [slice(None)] * 3
-        at[axis] = index
-        return tuple(at)
 
     def summand(ref, lanes, axis, where, half=None):
         at = [whole, whole, whole]
@@ -367,44 +377,44 @@
     offsets = [(m, k) for m in (2, 1, -1, 0) for k in (2, 1, -1, 0) if (m, k) != (0, 0)]
 
     class Scatter:
-        def __init__(self, h):
-            self.h = h
-            self.swap = dict(zip((2, 1, -1, 0), slots(4)))
-            self.far = [slots(2) for p in parts]
+        def __init__(self, h, direct):
+            self.h, self.direct = h, direct
+            self.swap = slots(2)
+            self.far = None if direct else [slots(2) for p in parts]
             self.last = slots(3)
             self.nexts = slots(3)
 
-        def down(self, o):
+        def down(self):
             h = self.h
-            for p, (lanes, (a, b, c)) in enumerate(SCATTER):
-                cut = slice(lanes[0], lanes[0] + lanes[1])
-                high = slice(HALF + lanes[0], HALF + lanes[0] + lanes[1])
-                rows = place(a, shifted(a, o))
-                x = h4[(h,) + rows + (slice(None), slice(None))].reshape(128, HIDDEN).astype(BF)
-                w = jnp.concatenate([weights[2 * HIDDEN :, cut], weights[2 * HIDDEN :, high]], axis=1)
-                y = jnp.dot(x, w, preferred_element_type=F32)
-                for half in range(2):
-                    piece = y[:, half * lanes[1] : (half + 1) * lanes[1]].reshape(4, 4, 8, lanes[1])
-                    ps[(h, half) + rows + (slice(None), cut)] = piece.astype(BF)
-                send(
-                    summand(ps.at[h, other], lanes, a, shifted(a, o)), summand(pin.at[h], lanes, a, shifted(a, o)),
-                    peer, csem, self.swap[o],
-                )
+            for whose, there in ((other, ps), (core, own_sum)):
+                lanes = pl.ds(pl.multiple_of(whose * HALF, 128), HALF)
+                for i in range(2):
+                    x = hid[h, i * 256 : (i + 1) * 256, :]
+                    y = jnp.dot(x, weights[2 * HIDDEN :, lanes], preferred_element_type=F32)
+                    there[h, 2 * i : 2 * i + 2] = y.reshape(2, 4, 4, 8, HALF).astype(there.dtype)
+                    if there is ps:
+                        rows = pl.ds(2 * i, 2)
+                        send(ps.at[h, rows], pin.at[h, rows], peer, csem, self.swap[i])
+
+        def swapped(self):
+            for i in range(2):
+                arrived(pin.at[self.h, pl.ds(2 * i, 2)], self.swap[i])
 
         def joined(self, p, o):
             h = self.h
             lanes, (a, b, c) = SCATTER[p]
             cut = slice(lanes[0], lanes[0] + lanes[1])
-            if p == 0:
-                arrived(pin.at[h, 0], self.swap[o])
             for i, j, at in cells(a, shifted(a, o)):
-                at = at + (slice(None), cut)
-                tot[(h,) + at] = (ps[(h, core) + at].astype(F32) + pin[(h,) + at].astype(F32)).astype(BF)
+                at = (h,) + at + (slice(None), cut)
+                tot[at] = (own_sum[at] + pin[at].astype(F32)).astype(BF)
 
         def open(self):
             h = self.h
             for p, (lanes, (a, b, c)) in enumerate(SCATTER):
                 self.joined(p, 2)
+                if self.direct:
+                    self.whole_chunk(p, 2, 2)
+                    continue
                 for way, k in enumerate((1, -1)):
                     send(
                         summand(tot.at[h], lanes, a, shifted(a, 2), halves[way]),
@@ -412,12 +422,23 @@
                         chip_at(a, k), csem, self.far[p][way],
                     )
 
+        def whole_chunk(self, p, k, way):
+            h = self.h
+            lanes, (a, b, c) = SCATTER[p]
+            send(
+                summand(tot.at[h], lanes, a, shifted(a, k)), fin.at[h, way, :, :, :, pl.ds(lanes[0], lanes[1])],
+                chip_at(a, k), csem, self.last[p],
+            )
+
         def near(self, k):
             h = self.h
             way = 0 if k == 1 else 1
             half = halves[1 - way]
             for p, (lanes, (a, b, c)) in enumerate(SCATTER):
                 self.joined(p, k)
+                if self.direct:
+                    self.whole_chunk(p, k, way)
+                    continue
                 send(
                     summand(tot.at[h], lanes, a, shifted(a, k), half),
                     fin.at[h, way, half, :, :, pl.ds(lanes[0], lanes[1])],
@@ -450,13 +471,13 @@
             for p, (lanes, (a, b, c)) in enumerate(SCATTER):
                 cut = slice(lanes[0], lanes[0] + lanes[1])
                 lanes_ds = pl.ds(lanes[0], lanes[1])
-                arrived(fin.at[h, :, :, :, :, lanes_ds], self.last[p])
+                count = 3 if self.direct else 2
+                arrived(fin.at[h, 0:count, :, :, :, lanes_ds], self.last[p])
                 for i, j, at in cells(a, me[a]):
-                    t1[h, i, j, :, cut] = (
-                        tot[(h,) + at + (slice(None), cut)].astype(F32)
-                        + fin[h, 0, i, j, :, cut].astype(F32)
-                        + fin[h, 1, i, j, :, cut].astype(F32)
-                    ).astype(BF)
+                    sum_ = tot[(h,) + at + (slice(None), cut)].astype(F32)
+                    for n in range(count):
+                        sum_ += fin[h, n, i, j, :, cut].astype(F32)
+                    t1[h, i, j, :, cut] = sum_.astype(BF)
                 d, e = [axis for axis in range(3) if axis != a]
                 for n, (m, k) in enumerate(offsets):
                     send(
@@ -475,69 +496,105 @@
                     sum_ += r2[h, n, :, cut].astype(F32)
                 res[h, :, cut] = sum_.astype(BF)
 
-    phase("gather1")
-    ga, gb = Gather(0), Gather(1)
-    sa, sb = Scatter(0), Scatter(1)
+    ga, gb = Gather(0, DIRECT[0]), Gather(1, DIRECT[1])
+    sa, sb = Scatter(0, DIRECT[2]), Scatter(1, DIRECT[3])
+    phase("attend_a")
+    attend(0)
+    attend(1)
+    phase("project_a")
+    base = pl.multiple_of(core * 48, 16)
+    loads = (
+        (eg_h, 0, 448), (dg_h.at[pl.ds(base, 64)], 448, 64),
+        (eu_h, 512, 448), (du_h.at[pl.ds(base, 64)], 960, 64),
+        (ed_h, 1024, 448), (dd_h.at[pl.ds(base, 64)], 1472, 64),
+    )
+    for src, row, count in loads:
+        pltpu.make_async_copy(src, weights.at[pl.ds(row, count)], wsem).start()
+    pltpu.make_async_copy(wo, wo, so).wait()
+    project(0)
+    pl.semaphore_wait(barrier, 37)
+    pair(0)
+    phase("attend_b1")
+    attend(2)
+    phase("norm_a")
+    norm_half(0)
     ga.plane()
+    phase("attend_b2")
+    attend(3)
+    phase("project_b")
+    project(1)
+    pair(1)
+    wk_copy.wait()
+    wv_copy.wait()
+    nk[...] = jnp.dot(normed_all, wk[...], preferred_element_type=F32).astype(BF)
+    nv[...] = jnp.dot(normed_all, wv[...], preferred_element_type=F32).astype(BF)
+    phase("norm_b")
+    norm_half(1)
     gb.plane()
-    phase("gather2")
+    phase("rounds_a")
     ga.rounds()
-    phase("gather3")
-    ga.relay(0)
+    phase("relay_a")
+    if not ga.direct:
+        ga.relay(0)
+    phase("rounds_b")
     gb.rounds()
-    phase("gather4")
-    for o in steps:
-        ga.relay(o)
-    gb.relay(0)
+    phase("relay_a2")
+    if not ga.direct:
+        for o in steps:
+            ga.relay(o)
     ga.neighbours()
-    phase("gather5")
-    for o in steps:
-        gb.relay(o)
+    phase("relay_b")
+    if not gb.direct:
+        for o in (0, *steps):
+            gb.relay(o)
+    phase("farthest_a")
     ga.farthest()
     pltpu.make_async_copy(weights, weights, wsem).wait()
     ga.complete()
     phase("hidden_a")
     hidden_unit(0, 0, 0)
     hidden_unit(0, 0, 1)
+    phase("neighbours_b")
     gb.neighbours()
+    phase("hidden_a2")
     hidden_unit(0, 1, 0)
     hidden_unit(0, 1, 1)
     phase("down_a")
-    sa.down(2)
     gb.farthest()
-    sa.down(1)
-    sa.open()
-    sa.down(-1)
-    sa.near(1)
-    sa.down(0)
-    sa.near(-1)
+    sa.down()
     phase("complete_b")
     gb.complete()
+    hidden_unit(1, 0, 0)
+    phase("swap_a")
+    sa.swapped()
+    sa.open()
+    sa.near(1)
+    sa.near(-1)
     phase("hidden_b")
-    hidden_unit(1, 0, 0)
+    hidden_unit(1, 0, 1)
     sa.own()
-    hidden_unit(1, 0, 1)
-    sa.close()
     hidden_unit(1, 1, 0)
     hidden_unit(1, 1, 1)
+    phase("close_a")
+    if not sa.direct:
+        sa.close()
     phase("down_b")
-    sb.down(2)
-    sb.down(1)
+    sb.down()
+    phase("swap_b")
+    sb.swapped()
     sb.open()
+    sb.near(1)
+    sb.near(-1)
     phase("plane_a")
     sa.plane()
-    phase("near_b")
-    sb.down(-1)
-    sb.near(1)
-    sb.down(0)
-    sb.near(-1)
     phase("close_b")
-    sb.close()
+    if not sb.direct:
+        sb.close()
     sb.own()
+    phase("plane_b")
+    sb.plane()
     phase("total_a")
     sa.total()
-    phase("plane_b")
-    sb.plane()
     phase("total_b")
     sb.total()
     phase("exchange")
@@ -550,7 +607,7 @@
     assert used[0] == N_RECV, used[0]
     rows = gath.reshape(2048, WIDE).at[pl.ds(0, 2032)]
     pltpu.make_async_copy(rows, rows, gsem).wait()
-    rows = ps.reshape(2048, HALF).at[pl.ds(0, 2040)]
+    rows = ckv.reshape(2 * SEQS * CACHE, 128).at[pl.ds(0, 2040 * 8)]
     pltpu.make_async_copy(rows, rows, csem).wait()
     pltpu.make_async_copy(part, part, psem).wait()
     phase(None)
@@ -574,9 +631,18 @@
     return pl.pallas_call(
         layer_kernel,
         out_shape=(jax.ShapeDtypeStruct((2, 8, HALF), BF),) + OUT_SHAPES[1:],
-        in_specs=[VM] * 3 + [pl.BlockSpec(memory_space=pltpu.SMEM)] + [VM] * 4 + [HB] * 12,
+        in_specs=[HB] * 20,
         out_specs=(VM, VM, VM),
         scratch_shapes=[
+            pltpu.VMEM((2, 8, D), BF),
+            pltpu.VMEM((1, D), F32),
+            pltpu.VMEM((1, HEADS), F32),
+            pltpu.SMEM((SEQS,), jnp.int32),
+            pltpu.VMEM((1, D), F32),
+            pltpu.VMEM((D,), BF),
+            pltpu.VMEM((2, 8), jnp.int32),
+            pltpu.VMEM((2, 8), BF),
+            pltpu.SemaphoreType.DMA((8,)),
             pltpu.VMEM((D, 1024), BF),
             pltpu.VMEM((D, 128), BF),
             pltpu.VMEM((D, 128), BF),
@@ -589,12 +655,13 @@
             pltpu.VMEM((2, 8, HALF), F32),
             pltpu.VMEM((2, 2, 4, 4, 4, 8, WIDE), BF),
             pltpu.VMEM((3 * HIDDEN, D), BF),
-            pltpu.VMEM((2, 512, HIDDEN), F32),
-            pltpu.VMEM((2, 2, 4, 4, 4, 8, HALF), BF),
+            pltpu.VMEM((2, 512, HIDDEN), BF),
+            pltpu.VMEM((2, 4, 4, 4, 8, HALF), BF),
+            pltpu.VMEM((2, 4, 4, 4, 8, HALF), F32),
             pltpu.VMEM((2, 4, 4, 4, 8, HALF), BF),
             pltpu.VMEM((2, 4, 4, 4, 8, HALF), BF),
             pltpu.VMEM((2, 2, 2, 4, 8, HALF), BF),
-            pltpu.VMEM((2, 2, 4, 4, 8, HALF), BF),
+            pltpu.VMEM((2, 3, 4, 4, 8, HALF), BF),
             pltpu.VMEM((2, 4, 4, 8, HALF), BF),
             pltpu.VMEM((2, 15, 8, HALF), BF),
             pltpu.VMEM((2, 8, HALF), BF),
@@ -610,7 +677,7 @@
             pltpu.SemaphoreType.DMA((N_RECV,)),
         ],
         compiler_params=pltpu.CompilerParams(
-            vmem_limit_bytes=63 * 1024 * 1024, collective_id=0, has_side_effects=True
+            vmem_limit_bytes=67043328, collective_id=0, has_side_effects=True
         ),
         name="layer",
     )(*args)

time: 60.3 us -> 55 us (0.912)
  Pallas kernels: 59.4 us -> 54.2 us
    pallas_call x1, Pallas kernels: 58 us -> 52.8 us  [layer(): pl.pallas_call(layer_kernel, out_shape=(jax.ShapeDtypeStruct((2, 8, HALF)...]
where the time goes in v1:
time: 55 us; the launch traced here: 54.9 us
  Pallas kernels  54.2 us (99%)
  between operations  0.65 us (1%)
    pallas_call x1, Pallas kernels, layer(): pl.pallas_call(layer_kernel, out_shape=(jax.ShapeDtypeStruct((2, 8, HALF)...  52.8 us
    pallas_call x1, Pallas kernels, shards(): pl.pallas_call(finish_kernel, out_shape=OUT_SHAPES, in_specs=[VM] * 3, ou...  1.39 us

profile of v1, /device:TPU:1, one launch (start us, length us, event | category | flops | bytes accessed | tf_op | source)
XLA Modules:
  0.0 54.9 jit_solution(4317987751499947107)
XLA Ops:
  0.6 52.8 %layer.1 = (bf16[2,8,1024]{2,1,0:T(8,128)(2,1)}, bf16[16,128]{1,0:T(8,128)(2,1)}, bf16[16,128]{1,0:T(8,128)(2,1)}) custom-call(bf16[2,8,2048]{2,1,0:T(8,128)(2,1)} %bitcast.14, f32[1,2048]{1,0:T(1,128)} %bitcast.15, f32[1,16]{1,0:T(1,128)} %bitcast.18, s32[16]{0:T(128)} %lengths_h.1, f32[1,2048]{1,0:T(1,128)} %bitcast.16, bf16[2048]{0:T(1024)(128)(2,1)} %mix_h.1, ...), custom_call_target="tpu_custom_call" | custom-call | tf_op jit(solution)/shard_map/layer/pallas_call | solution.py:631
  53.5 1.4 %finish.1 = (bf16[8,2048]{1,0:T(8,128)(2,1)}, bf16[16,128]{1,0:T(8,128)(2,1)}, bf16[16,128]{1,0:T(8,128)(2,1)}) custom-call(bf16[2,8,1024]{2,1,0:T(8,128)(2,1)} %get-tuple-element.6.a, bf16[16,128]{1,0:T(8,128)(2,1)} %get-tuple-element.7.b, bf16[16,128]{1,0:T(8,128)(2,1)} %get-tuple-element.8.c), custom_call_target="tpu_custom_call" | custom-call | tf_op jit(solution)/shard_map/finish/pallas_call | solution.py:697

commit v2 on v1

--- a/solution.py
+++ b/solution.py
@@ -37,8 +37,7 @@
 SCATTER = (((0, 384), (0, 1, 2)), ((384, 384), (2, 0, 1)), ((768, 256), (1, 2, 0)))
 HIDDEN = 512
 GROUP = 4
-DIRECT = (True, True, True, True)
-N_RECV = 99 - 12 * sum(DIRECT[0:2]) - 6 * sum(DIRECT[2:4])
+N_RECV = 54
 PHASE = [None]
 
 
@@ -56,7 +55,7 @@
     out, nk, nv,
     tokens, norm, bias, lengths, gain, mix_w, routes, route_w, small,
     wq, wk, wv, wo, ckv, qs, xs, part,
-    rx, mid, gath, weights, hid, ps, own_sum, pin, tot, rb, fin, t1, r2, res, got,
+    rx, mid, gath, weights, hid, ps, own_sum, pin, tot, fin, t1, r2, ex,
     sq, skv, so, sw, wsem, psem, gsem, csem, rsem,
 ):
     phase("start")
@@ -113,10 +112,13 @@
     pl.semaphore_signal(barrier, inc=1, device_id=peer, device_id_type=MESH)
     for axis in range(3):
         for k in range(1, 4):
-            pl.semaphore_signal(barrier, inc=1, device_id=chip_at(axis, k), device_id_type=MESH)
+            target = chip_at(axis, k)
+            pl.semaphore_signal(barrier, inc=1, device_id=target, device_id_type=MESH)
+            pl.semaphore_signal(barrier, inc=1, device_id=(target[0], other), device_id_type=MESH)
             for m in range(1, 4):
                 target = chip_at(axis, k, (axis + 1) % 3, m)
                 pl.semaphore_signal(barrier, inc=1, device_id=target, device_id_type=MESH)
+                pl.semaphore_signal(barrier, inc=1, device_id=(target[0], other), device_id_type=MESH)
 
     for copy in littles[:4]:
         copy.wait()
@@ -235,7 +237,7 @@
         mix_high = mix.astype(BF).astype(F32)
         meta = jnp.where(kind == 8, mix_high, summed[:, D : D + 128])
         meta = jnp.where(kind == 9, mix - mix_high, meta)
-        mid[h] = jnp.where(core == 0, middle[:, 0:HALF], middle[:, HALF:D])
+        mid[h] = middle
         own = jnp.where(core == 0, normed[:, 0:HALF], normed[:, HALF:D])
         gath[h, core, me[0], me[1], me[2], :, 0:HALF] = own.astype(BF)
         gath[h, core, me[0], me[1], me[2], :, HALF:WIDE] = meta.astype(BF)
@@ -243,27 +245,18 @@
     whole = pl.ds(0, 4)
     parts = range(3)
     steps = (1, -1, 2)
-    upward, downward = (0, 2), (1, -1)
     g2 = gath.reshape(2, 2, 512, WIDE)
 
-    def sized(rows, lanes):
-        return g2.at[0, 0, pl.ds(0, rows), pl.ds(lanes[0], lanes[1])]
+    def sized(rows):
+        return g2.at[0, 0, pl.ds(0, rows)]
 
     class Gather:
-        def __init__(self, h, direct):
-            self.h, self.direct = h, direct
-            self.first = slots(3)
-            self.second = [dict(zip(steps, slots(3))) for p in parts]
+        def __init__(self, h):
+            self.h = h
+            (self.first,) = slots(1)
+            self.second = dict(zip(steps, slots(3)))
             (self.across,) = slots(1)
-            if direct:
-                self.straight = [dict(zip(steps, slots(3))) for p in parts]
-                return
-            self.below = [dict(zip((0, 2, 1), slots(3))) for p in parts]
-            self.above = [dict(zip((1, -1, 0), slots(3))) for p in parts]
-            for p in parts:
-                self.below[p][-1] = self.below[p][1]
-                self.above[p][2] = self.above[p][0]
-            self.relayed = slots(3)
+            self.straight = {o: dict(zip(steps, slots(3))) for o in (0, *steps)}
 
         def held(self, lanes, where):
             at = [me[0], me[1], me[2]]
@@ -279,27 +272,22 @@
                 for k in (0, *steps):
                     for p, (lanes, (a, b, c)) in enumerate(GATHER):
                         if (k, m) != (0, 0):
-                            slot = self.second[p][m] if m else self.first[p]
+                            slot = self.second[m] if m else self.first
                             self.spread(self.held(lanes, {}), chip_at(a, k, b, m), slot)
 
-        def bulk(self, p, o):
-            lanes, (a, b, c) = GATHER[p]
+        def round(self, o):
             if o:
-                arrived(sized(32, lanes), self.second[p][-o if o != 2 else 2])
+                arrived(sized(32), self.second[-o if o != 2 else 2])
             else:
-                arrived(sized(24, lanes), self.first[p])
-            block = self.held(lanes, {a: whole, b: shifted(b, o)})
-            if self.direct:
-                for k in (2, 1, -1):
-                    self.spread(block, chip_at(c, k), self.straight[p][k])
-                return
-            self.spread(block, chip_at(c, 1), self.below[p][o])
-            self.spread(block, chip_at(c, -1), self.above[p][o])
+                arrived(sized(24), self.first)
+            for k in (2, 1, -1):
+                for p, (lanes, (a, b, c)) in enumerate(GATHER):
+                    block = self.held(lanes, {a: whole, b: shifted(b, o)})
+                    self.spread(block, chip_at(c, k), self.straight[o][k])
 
         def rounds(self):
             for o in (0, *steps):
-                for p in parts:
-                    self.bulk(p, o)
+                self.round(o)
             for p in parts:
                 self.hand_over(p, 0)
 
@@ -307,30 +295,12 @@
             lanes, (a, b, c) = GATHER[p]
             self.spread(self.held(lanes, {a: whole, b: whole, c: shifted(c, o)}), peer, self.across)
 
-        def relay(self, o):
-            for p, (lanes, (a, b, c)) in enumerate(GATHER):
-                below = o in upward
-                arrived(sized(32, lanes), (self.below if below else self.above)[p][o])
-                block = self.held(lanes, {a: whole, b: shifted(b, o), c: shifted(c, -1 if below else 1)})
-                self.spread(block, chip_at(c, 1 if below else -1), self.relayed[p])
-
-        def neighbours(self):
-            if self.direct:
-                for p, (lanes, _) in enumerate(GATHER):
-                    for k in (1, -1):
-                        arrived(sized(128, lanes), self.straight[p][k])
-                        self.hand_over(p, -k)
-                return
-            for p, (lanes, _) in enumerate(GATHER):
-                arrived(sized(64, lanes), self.below[p][1])
-                self.hand_over(p, -1)
-                arrived(sized(64, lanes), self.above[p][0])
-                self.hand_over(p, 1)
-
-        def farthest(self):
-            for p, (lanes, _) in enumerate(GATHER):
-                arrived(sized(128, lanes), self.straight[p][2] if self.direct else self.relayed[p])
-                self.hand_over(p, 2)
+        def came(self, o):
+            for k in (2, 1, -1):
+                arrived(sized(32), self.straight[o][k])
+                for lanes, (a, b, c) in GATHER:
+                    block = self.held(lanes, {a: whole, b: shifted(b, o), c: shifted(c, -k if k != 2 else 2)})
+                    self.spread(block, peer, self.across)
 
         def complete(self):
             arrived(g2.at[self.h, 0], self.across)
@@ -358,7 +328,6 @@
         u = product(HIDDEN + n * 256)
         hid[h, rows, n * 256 : (n + 1) * 256] = (g * jax.nn.sigmoid(g) * u * factor).astype(BF)
 
-    halves = (pl.ds(0, 2), pl.ds(2, 2))
 
     def summand(ref, lanes, axis, where, half=None):
         at = [whole, whole, whole]
@@ -377,28 +346,44 @@
     offsets = [(m, k) for m in (2, 1, -1, 0) for k in (2, 1, -1, 0) if (m, k) != (0, 0)]
 
     class Scatter:
-        def __init__(self, h, direct):
-            self.h, self.direct = h, direct
-            self.swap = slots(2)
-            self.far = None if direct else [slots(2) for p in parts]
+        def __init__(self, h, swaps):
+            self.h = h
+            self.swap = slots(swaps)
             self.last = slots(3)
             self.nexts = slots(3)
-
-        def down(self):
+            (self.cell,) = slots(1)
+
+        def down(self, early):
             h = self.h
-            for whose, there in ((other, ps), (core, own_sum)):
-                lanes = pl.ds(pl.multiple_of(whose * HALF, 128), HALF)
-                for i in range(2):
-                    x = hid[h, i * 256 : (i + 1) * 256, :]
-                    y = jnp.dot(x, weights[2 * HIDDEN :, lanes], preferred_element_type=F32)
-                    there[h, 2 * i : 2 * i + 2] = y.reshape(2, 4, 4, 8, HALF).astype(there.dtype)
-                    if there is ps:
-                        rows = pl.ds(2 * i, 2)
-                        send(ps.at[h, rows], pin.at[h, rows], peer, csem, self.swap[i])
-
-        def swapped(self):
-            for i in range(2):
-                arrived(pin.at[self.h, pl.ds(2 * i, 2)], self.swap[i])
+            if not early:
+                quarter = HALF // 2
+                for whose, there in ((other, ps), (core, own_sum)):
+                    for n in range(2):
+                        columns = pl.ds(pl.multiple_of(whose * HALF + n * quarter, 128), quarter)
+                        cut = slice(n * quarter, (n + 1) * quarter)
+                        for i in range(2):
+                            x = hid[h, i * 256 : (i + 1) * 256, :]
+                            y = jnp.dot(x, weights[2 * HIDDEN :, columns], preferred_element_type=F32)
+                            y = y.reshape(2, 4, 4, 8, quarter).astype(there.dtype)
+                            there[h, 2 * i : 2 * i + 2, :, :, :, cut] = y
+                            if there is ps:
+                                at = (pl.ds(2 * i, 2), whole, whole, slice(None), pl.ds(n * quarter, quarter))
+                                send(ps.at[(h,) + at], pin.at[(h,) + at], peer, csem, self.swap[0])
+                return
+            for p, (lanes, _) in enumerate(SCATTER):
+                cut = slice(lanes[0], lanes[0] + lanes[1])
+                for whose, there in ((other, ps), (core, own_sum)):
+                    columns = pl.ds(pl.multiple_of(whose * HALF + lanes[0], 128), lanes[1])
+                    for i in range(2):
+                        x = hid[h, i * 256 : (i + 1) * 256, :]
+                        y = jnp.dot(x, weights[2 * HIDDEN :, columns], preferred_element_type=F32)
+                        there[h, 2 * i : 2 * i + 2, :, :, :, cut] = y.reshape(2, 4, 4, 8, lanes[1]).astype(there.dtype)
+                        if there is ps:
+                            at = (pl.ds(2 * i, 2), whole, whole, slice(None), pl.ds(lanes[0], lanes[1]))
+                            send(ps.at[(h,) + at], pin.at[(h,) + at], peer, csem, self.swap[p])
+                if p:
+                    self.chunks(p - 1)
+            self.chunks(2)
 
         def joined(self, p, o):
             h = self.h
@@ -408,19 +393,13 @@
                 at = (h,) + at + (slice(None), cut)
                 tot[at] = (own_sum[at] + pin[at].astype(F32)).astype(BF)
 
-        def open(self):
-            h = self.h
-            for p, (lanes, (a, b, c)) in enumerate(SCATTER):
-                self.joined(p, 2)
-                if self.direct:
-                    self.whole_chunk(p, 2, 2)
-                    continue
-                for way, k in enumerate((1, -1)):
-                    send(
-                        summand(tot.at[h], lanes, a, shifted(a, 2), halves[way]),
-                        rb.at[h, way, :, :, :, pl.ds(lanes[0], lanes[1])],
-                        chip_at(a, k), csem, self.far[p][way],
-                    )
+        def chunks(self, p):
+            lanes = SCATTER[p][0]
+            if len(self.swap) > 1:
+                arrived(pin.at[self.h, :, :, :, :, pl.ds(lanes[0], lanes[1])], self.swap[p])
+            for k, way in ((2, 2), (1, 0), (-1, 1)):
+                self.joined(p, k)
+                self.whole_chunk(p, k, way)
 
         def whole_chunk(self, p, k, way):
             h = self.h
@@ -430,74 +409,49 @@
                 chip_at(a, k), csem, self.last[p],
             )
 
-        def near(self, k):
-            h = self.h
-            way = 0 if k == 1 else 1
-            half = halves[1 - way]
-            for p, (lanes, (a, b, c)) in enumerate(SCATTER):
-                self.joined(p, k)
-                if self.direct:
-                    self.whole_chunk(p, k, way)
-                    continue
-                send(
-                    summand(tot.at[h], lanes, a, shifted(a, k), half),
-                    fin.at[h, way, half, :, :, pl.ds(lanes[0], lanes[1])],
-                    chip_at(a, k), csem, self.last[p],
-                )
-
-        def close(self):
-            h = self.h
-            for p, (lanes, (a, b, c)) in enumerate(SCATTER):
-                cut = slice(lanes[0], lanes[0] + lanes[1])
-                lanes_ds = pl.ds(lanes[0], lanes[1])
-                for way, k in enumerate((1, -1)):
-                    arrived(rb.at[h, way, :, :, :, lanes_ds], self.far[p][way])
-                    for i, j, at in cells(a, shifted(a, k)):
-                        if i // 2 == way:
-                            at = (h,) + at + (slice(None), cut)
-                            tot[at] = (tot[at].astype(F32) + rb[h, way, i % 2, j, :, cut].astype(F32)).astype(BF)
-                    send(
-                        summand(tot.at[h], lanes, a, shifted(a, k), halves[way]),
-                        fin.at[h, way, halves[way], :, :, lanes_ds],
-                        chip_at(a, k), csem, self.last[p],
-                    )
-
-        def own(self):
-            for p in parts:
-                self.joined(p, 0)
-
         def plane(self):
             h = self.h
             for p, (lanes, (a, b, c)) in enumerate(SCATTER):
                 cut = slice(lanes[0], lanes[0] + lanes[1])
                 lanes_ds = pl.ds(lanes[0], lanes[1])
-                count = 3 if self.direct else 2
-                arrived(fin.at[h, 0:count, :, :, :, lanes_ds], self.last[p])
+                arrived(fin.at[h, :, :, :, :, lanes_ds], self.last[p])
                 for i, j, at in cells(a, me[a]):
-                    sum_ = tot[(h,) + at + (slice(None), cut)].astype(F32)
-                    for n in range(count):
+                    at = (h,) + at + (slice(None), cut)
+                    sum_ = own_sum[at] + pin[at].astype(F32)
+                    for n in range(3):
                         sum_ += fin[h, n, i, j, :, cut].astype(F32)
                     t1[h, i, j, :, cut] = sum_.astype(BF)
                 d, e = [axis for axis in range(3) if axis != a]
                 for n, (m, k) in enumerate(offsets):
                     send(
-                        t1.at[h, shifted(d, m), shifted(e, k), :, lanes_ds], r2.at[h, n, :, lanes_ds],
-                        chip_at(d, m, e, k), csem, self.nexts[p],
+                        t1.at[h, shifted(d, m), shifted(e, k), :, lanes_ds], r2.at[core, n, :, lanes_ds],
+                        (chip_at(d, m, e, k)[0], h), csem, self.nexts[p],
                     )
+
+                @pl.when(core != h)
+                def _():
+                    send(t1.at[h, me[d], me[e], :, lanes_ds], ex.at[:, lanes_ds], peer, csem, self.cell)
 
         def total(self):
             h = self.h
-            for p, (lanes, (a, b, c)) in enumerate(SCATTER):
-                cut = slice(lanes[0], lanes[0] + lanes[1])
-                arrived(r2.at[h, :, :, pl.ds(lanes[0], lanes[1])], self.nexts[p])
-                d, e = [axis for axis in range(3) if axis != a]
-                sum_ = mid[h, :, cut] + t1[h, me[d], me[e], :, cut].astype(F32)
-                for n in range(15):
-                    sum_ += r2[h, n, :, cut].astype(F32)
-                res[h, :, cut] = sum_.astype(BF)
-
-    ga, gb = Gather(0, DIRECT[0]), Gather(1, DIRECT[1])
-    sa, sb = Scatter(0, DIRECT[2]), Scatter(1, DIRECT[3])
+
+            @pl.when(core == h)
+            def _():
+                arrived(ex, self.cell)
+                for p, (lanes, (a, b, c)) in enumerate(SCATTER):
+                    cut = slice(lanes[0], lanes[0] + lanes[1])
+                    arrived(r2.at[:, :, :, pl.ds(lanes[0], lanes[1])], self.nexts[p])
+                    d, e = [axis for axis in range(3) if axis != a]
+                    for half in range(2):
+                        there = slice(half * HALF + lanes[0], half * HALF + lanes[0] + lanes[1])
+                        own = t1[h, me[d], me[e], :, cut] if half == h else ex[:, cut]
+                        sum_ = mid[h, :, there] + own.astype(F32)
+                        for n in range(15):
+                            sum_ += r2[half, n, :, cut].astype(F32)
+                        out[:, there] = sum_.astype(BF)
+
+    ga, gb = Gather(0), Gather(1)
+    sa, sb = Scatter(0, 1), Scatter(1, 3)
     phase("attend_a")
     attend(0)
     attend(1)
@@ -512,7 +466,7 @@
         pltpu.make_async_copy(src, weights.at[pl.ds(row, count)], wsem).start()
     pltpu.make_async_copy(wo, wo, so).wait()
     project(0)
-    pl.semaphore_wait(barrier, 37)
+    pl.semaphore_wait(barrier, 73)
     pair(0)
     phase("attend_b1")
     attend(2)
@@ -524,85 +478,58 @@
     phase("project_b")
     project(1)
     pair(1)
+    phase("norm_b")
+    norm_half(1)
+    gb.plane()
+    phase("rounds_a")
     wk_copy.wait()
     wv_copy.wait()
     nk[...] = jnp.dot(normed_all, wk[...], preferred_element_type=F32).astype(BF)
     nv[...] = jnp.dot(normed_all, wv[...], preferred_element_type=F32).astype(BF)
-    phase("norm_b")
-    norm_half(1)
-    gb.plane()
-    phase("rounds_a")
     ga.rounds()
-    phase("relay_a")
-    if not ga.direct:
-        ga.relay(0)
     phase("rounds_b")
     gb.rounds()
-    phase("relay_a2")
-    if not ga.direct:
-        for o in steps:
-            ga.relay(o)
-    ga.neighbours()
-    phase("relay_b")
-    if not gb.direct:
-        for o in (0, *steps):
-            gb.relay(o)
+    phase("neighbours_a")
+    for o in (0, 1, -1):
+        ga.came(o)
     phase("farthest_a")
-    ga.farthest()
+    ga.came(2)
     pltpu.make_async_copy(weights, weights, wsem).wait()
     ga.complete()
     phase("hidden_a")
     hidden_unit(0, 0, 0)
     hidden_unit(0, 0, 1)
+    hidden_unit(0, 1, 0)
     phase("neighbours_b")
-    gb.neighbours()
+    for o in (0, 1, -1):
+        gb.came(o)
     phase("hidden_a2")
-    hidden_unit(0, 1, 0)
     hidden_unit(0, 1, 1)
+    gb.came(2)
     phase("down_a")
-    gb.farthest()
-    sa.down()
+    sa.down(False)
     phase("complete_b")
     gb.complete()
+    phase("hidden_b1")
     hidden_unit(1, 0, 0)
     phase("swap_a")
-    sa.swapped()
-    sa.open()
-    sa.near(1)
-    sa.near(-1)
+    arrived(pin.at[0], sa.swap[0])
+    for p in parts:
+        sa.chunks(p)
     phase("hidden_b")
     hidden_unit(1, 0, 1)
-    sa.own()
     hidden_unit(1, 1, 0)
     hidden_unit(1, 1, 1)
-    phase("close_a")
-    if not sa.direct:
-        sa.close()
     phase("down_b")
-    sb.down()
-    phase("swap_b")
-    sb.swapped()
-    sb.open()
-    sb.near(1)
-    sb.near(-1)
+    sb.down(True)
     phase("plane_a")
     sa.plane()
-    phase("close_b")
-    if not sb.direct:
-        sb.close()
-    sb.own()
     phase("plane_b")
     sb.plane()
     phase("total_a")
     sa.total()
     phase("total_b")
     sb.total()
-    phase("exchange")
-    (slot,) = slots(1)
-    send(res.at[other], got, peer, csem, slot)
-    out[core] = res[core]
-    arrived(got, slot)
-    out[other] = got[...]
     phase("finish")
     assert used[0] == N_RECV, used[0]
     rows = gath.reshape(2048, WIDE).at[pl.ds(0, 2032)]
@@ -614,8 +541,7 @@
 
 
 def finish_kernel(a, b, c, out, nk, nv):
-    out[:, 0:HALF] = a[0]
-    out[:, HALF:D] = a[1]
+    out[...] = a[...]
     nk[...] = b[...]
     nv[...] = c[...]
 
@@ -630,7 +556,7 @@
 def layer(*args):
     return pl.pallas_call(
         layer_kernel,
-        out_shape=(jax.ShapeDtypeStruct((2, 8, HALF), BF),) + OUT_SHAPES[1:],
+        out_shape=OUT_SHAPES,
         in_specs=[HB] * 20,
         out_specs=(VM, VM, VM),
         scratch_shapes=[
@@ -652,7 +578,7 @@
             pltpu.VMEM((SEQS, 8, 128), F32),
             pltpu.VMEM((2, 8, D + 128), BF),
             pltpu.VMEM((2, 8, D + 128), BF),
-            pltpu.VMEM((2, 8, HALF), F32),
+            pltpu.VMEM((2, 8, D), F32),
             pltpu.VMEM((2, 2, 4, 4, 4, 8, WIDE), BF),
             pltpu.VMEM((3 * HIDDEN, D), BF),
             pltpu.VMEM((2, 512, HIDDEN), BF),
@@ -660,11 +586,9 @@
             pltpu.VMEM((2, 4, 4, 4, 8, HALF), F32),
             pltpu.VMEM((2, 4, 4, 4, 8, HALF), BF),
             pltpu.VMEM((2, 4, 4, 4, 8, HALF), BF),
-            pltpu.VMEM((2, 2, 2, 4, 8, HALF), BF),
             pltpu.VMEM((2, 3, 4, 4, 8, HALF), BF),
             pltpu.VMEM((2, 4, 4, 8, HALF), BF),
             pltpu.VMEM((2, 15, 8, HALF), BF),
-            pltpu.VMEM((2, 8, HALF), BF),
             pltpu.VMEM((8, HALF), BF),
             pltpu.SemaphoreType.DMA((4,)),
             pltpu.SemaphoreType.DMA((4,)),

time: 55 us -> 51.8 us (0.942)
  Pallas kernels: 54.2 us -> 51 us
    pallas_call x1, Pallas kernels: 52.8 us -> 49.6 us  [layer(): pl.pallas_call(layer_kernel, out_shape=OUT_SHAPES, in_specs=[HB] * 20, ou...]
where the time goes in v2:
time: 51.8 us; the launch traced here: 51.6 us
  Pallas kernels  51 us (98%)
  between operations  0.65 us (1%)
    pallas_call x1, Pallas kernels, layer(): pl.pallas_call(layer_kernel, out_shape=OUT_SHAPES, in_specs=[HB] * 20, ou...  49.6 us
    pallas_call x1, Pallas kernels, shards(): pl.pallas_call(finish_kernel, out_shape=OUT_SHAPES, in_specs=[VM] * 3, ou...  1.39 us

profile of v2, /device:TPU:1, one launch (start us, length us, event | category | flops | bytes accessed | tf_op | source)
XLA Modules:
  0.0 51.6 jit_solution(17671764463957267017)
XLA Ops:
  0.6 49.6 %layer.1 = (bf16[8,2048]{1,0:T(8,128)(2,1)}, bf16[16,128]{1,0:T(8,128)(2,1)}, bf16[16,128]{1,0:T(8,128)(2,1)}) custom-call(bf16[2,8,2048]{2,1,0:T(8,128)(2,1)} %bitcast.14, f32[1,2048]{1,0:T(1,128)} %bitcast.15, f32[1,16]{1,0:T(1,128)} %bitcast.18, s32[16]{0:T(128)} %lengths_h.1, f32[1,2048]{1,0:T(1,128)} %bitcast.16, bf16[2048]{0:T(1024)(128)(2,1)} %mix_h.1, ...), custom_call_target="tpu_custom_call" | custom-call | tf_op jit(solution)/shard_map/layer/pallas_call | solution.py:557
  50.2 1.4 %finish.1 = (bf16[8,2048]{1,0:T(8,128)(2,1)}, bf16[16,128]{1,0:T(8,128)(2,1)}, bf16[16,128]{1,0:T(8,128)(2,1)}) custom-call(bf16[8,2048]{1,0:T(8,128)(2,1)} %get-tuple-element.6.a, bf16[16,128]{1,0:T(8,128)(2,1)} %get-tuple-element.7.b, bf16[16,128]{1,0:T(8,128)(2,1)} %get-tuple-element.8.c), custom_call_target="tpu_custom_call" | custom-call | tf_op jit(solution)/shard_map/finish/pallas_call | solution.py:621

commit v3 on v2

--- a/solution.py
+++ b/solution.py
@@ -55,7 +55,7 @@
     out, nk, nv,
     tokens, norm, bias, lengths, gain, mix_w, routes, route_w, small,
     wq, wk, wv, wo, ckv, qs, xs, part,
-    rx, mid, gath, weights, hid, ps, own_sum, pin, tot, fin, t1, r2, ex,
+    rx, mid, gath, weights, hid, acc, ps, own_sum, pin, tot, fin, t1, r2, ex,
     sq, skv, so, sw, wsem, psem, gsem, csem, rsem,
 ):
     phase("start")
@@ -137,13 +137,11 @@
     query = jnp.zeros((SEQS, HEADS * 64), F32)
     for i in range(4):
         q_copy(i).wait()
-        if i == 1:
+        if i == 0:
+            cache_start(1)
+        elif i == 1:
             output_start()
-        else:
-            cache_start((1, 0, 2, 3)[i])
         query += jnp.dot(normed_all[:, i * 512 : (i + 1) * 512], wq[pl.ds(i * 512, 512), :], preferred_element_type=F32)
-    wk_copy.start()
-    wv_copy.start()
     query = query.astype(BF).astype(F32) * 0.125
     lane = lax.broadcasted_iota(jnp.int32, (SEQS, 128), 1)
     for i in range(8):
@@ -169,6 +167,8 @@
     def attend(i):
         group = [i * GROUP + j for j in range(GROUP)]
         cache_wait(i)
+        if i < 2:
+            cache_start(i + 2)
         scores = [
             lax.dot_general(qs[b].astype(BF), ck[b], NT, preferred_element_type=F32) + bias_col for b in group
         ]
@@ -268,8 +268,8 @@
             send(block, block, device, gsem, slot)
 
         def plane(self):
-            for m in (0, *steps):
-                for k in (0, *steps):
+            for m in (2, 1, -1, 0):
+                for k in (2, 1, -1, 0):
                     for p, (lanes, (a, b, c)) in enumerate(GATHER):
                         if (k, m) != (0, 0):
                             slot = self.second[m] if m else self.first
@@ -286,7 +286,7 @@
                     self.spread(block, chip_at(c, k), self.straight[o][k])
 
         def rounds(self):
-            for o in (0, *steps):
+            for o in (2, 1, -1, 0):
                 self.round(o)
             for p in parts:
                 self.hand_over(p, 0)
@@ -310,9 +310,19 @@
     dense_own = jnp.logical_and(column >= 448, jnp.logical_or(core == 0, column >= 464))
     kinds = lax.broadcasted_iota(jnp.int32, (256, 128), 1)
 
-    def hidden_unit(h, i, n):
+    def lane_product(h, whose, i, row):
+        lanes = pl.ds(pl.multiple_of(whose * HALF, 128), HALF)
+        x = g2[h, whose, i * 256 : (i + 1) * 256, 0:HALF]
+        return lax.dot_general(x, weights[row : row + 256, lanes], NT, preferred_element_type=F32)
+
+    def own_lanes(h):
+        for i in range(2):
+            for n in range(2):
+                for kind_of in range(2):
+                    acc[i, n, kind_of] = lane_product(h, core, i, kind_of * HIDDEN + n * 256)
+
+    def hidden_unit(h, i, n, begun=False):
         rows = slice(i * 256, (i + 1) * 256)
-        x = [g2[h, c, rows, 0:HALF] for c in range(2)]
         info = g2[h, 0, rows, HALF:WIDE].astype(F32)
         factor = jnp.sum(jnp.where(kinds == expert, info, 0.0), axis=1, keepdims=True)
         if n == 1:
@@ -320,12 +330,17 @@
             factor = jnp.where(column < 448, factor, jnp.where(dense_own, mixed, 0.0))
 
         def product(row):
+            x = [g2[h, c, rows, 0:HALF] for c in range(2)]
             w = weights[row : row + 256, :]
             y = lax.dot_general(x[0], w[:, 0:HALF], NT, preferred_element_type=F32)
             return y + lax.dot_general(x[1], w[:, HALF:D], NT, preferred_element_type=F32)
 
-        g = product(n * 256)
-        u = product(HIDDEN + n * 256)
+        if begun:
+            g = acc[i, n, 0] + lane_product(h, other, i, n * 256)
+            u = acc[i, n, 1] + lane_product(h, other, i, HIDDEN + n * 256)
+        else:
+            g = product(n * 256)
+            u = product(HIDDEN + n * 256)
         hid[h, rows, n * 256 : (n + 1) * 256] = (g * jax.nn.sigmoid(g) * u * factor).astype(BF)
 
 
@@ -361,26 +376,21 @@
                     for n in range(2):
                         columns = pl.ds(pl.multiple_of(whose * HALF + n * quarter, 128), quarter)
                         cut = slice(n * quarter, (n + 1) * quarter)
-                        for i in range(2):
-                            x = hid[h, i * 256 : (i + 1) * 256, :]
-                            y = jnp.dot(x, weights[2 * HIDDEN :, columns], preferred_element_type=F32)
-                            y = y.reshape(2, 4, 4, 8, quarter).astype(there.dtype)
-                            there[h, 2 * i : 2 * i + 2, :, :, :, cut] = y
-                            if there is ps:
-                                at = (pl.ds(2 * i, 2), whole, whole, slice(None), pl.ds(n * quarter, quarter))
-                                send(ps.at[(h,) + at], pin.at[(h,) + at], peer, csem, self.swap[0])
+                        y = jnp.dot(hid[h], weights[2 * HIDDEN :, columns], preferred_element_type=F32)
+                        there[h, :, :, :, :, cut] = y.reshape(4, 4, 4, 8, quarter).astype(there.dtype)
+                        if there is ps:
+                            at = (h, whole, whole, whole, slice(None), pl.ds(n * quarter, quarter))
+                            send(ps.at[at], pin.at[at], peer, csem, self.swap[0])
                 return
             for p, (lanes, _) in enumerate(SCATTER):
                 cut = slice(lanes[0], lanes[0] + lanes[1])
                 for whose, there in ((other, ps), (core, own_sum)):
                     columns = pl.ds(pl.multiple_of(whose * HALF + lanes[0], 128), lanes[1])
-                    for i in range(2):
-                        x = hid[h, i * 256 : (i + 1) * 256, :]
-                        y = jnp.dot(x, weights[2 * HIDDEN :, columns], preferred_element_type=F32)
-                        there[h, 2 * i : 2 * i + 2, :, :, :, cut] = y.reshape(2, 4, 4, 8, lanes[1]).astype(there.dtype)
-                        if there is ps:
-                            at = (pl.ds(2 * i, 2), whole, whole, slice(None), pl.ds(lanes[0], lanes[1]))
-                            send(ps.at[(h,) + at], pin.at[(h,) + at], peer, csem, self.swap[p])
+                    y = jnp.dot(hid[h], weights[2 * HIDDEN :, columns], preferred_element_type=F32)
+                    there[h, :, :, :, :, cut] = y.reshape(4, 4, 4, 8, lanes[1]).astype(there.dtype)
+                    if there is ps:
+                        at = (h, whole, whole, whole, slice(None), pl.ds(lanes[0], lanes[1]))
+                        send(ps.at[at], pin.at[at], peer, csem, self.swap[p])
                 if p:
                     self.chunks(p - 1)
             self.chunks(2)
@@ -464,6 +474,8 @@
     )
     for src, row, count in loads:
         pltpu.make_async_copy(src, weights.at[pl.ds(row, count)], wsem).start()
+    wk_copy.start()
+    wv_copy.start()
     pltpu.make_async_copy(wo, wo, so).wait()
     project(0)
     pl.semaphore_wait(barrier, 73)
@@ -490,22 +502,25 @@
     phase("rounds_b")
     gb.rounds()
     phase("neighbours_a")
-    for o in (0, 1, -1):
+    for o in (2, 1, -1):
         ga.came(o)
     phase("farthest_a")
-    ga.came(2)
+    ga.came(0)
     pltpu.make_async_copy(weights, weights, wsem).wait()
+    phase("own_lanes")
+    own_lanes(0)
+    phase("complete_a")
     ga.complete()
     phase("hidden_a")
-    hidden_unit(0, 0, 0)
-    hidden_unit(0, 0, 1)
-    hidden_unit(0, 1, 0)
+    hidden_unit(0, 0, 0, True)
+    gb.came(2)
+    hidden_unit(0, 0, 1, True)
+    gb.came(1)
+    hidden_unit(0, 1, 0, True)
+    hidden_unit(0, 1, 1, True)
     phase("neighbours_b")
-    for o in (0, 1, -1):
-        gb.came(o)
-    phase("hidden_a2")
-    hidden_unit(0, 1, 1)
-    gb.came(2)
+    gb.came(-1)
+    gb.came(0)
     phase("down_a")
     sa.down(False)
     phase("complete_b")
@@ -582,6 +597,7 @@
             pltpu.VMEM((2, 2, 4, 4, 4, 8, WIDE), BF),
             pltpu.VMEM((3 * HIDDEN, D), BF),
             pltpu.VMEM((2, 512, HIDDEN), BF),
+            pltpu.VMEM((2, 2, 2, 256, 256), F32),
             pltpu.VMEM((2, 4, 4, 4, 8, HALF), BF),
             pltpu.VMEM((2, 4, 4, 4, 8, HALF), F32),
             pltpu.VMEM((2, 4, 4, 4, 8, HALF), BF),

time: 51.8 us -> 51.5 us (level)
  no operation moved by 1% of the time
where the time goes in v3:
time: 51.5 us; the launch traced here: 51.3 us
  Pallas kernels  50.6 us (98%)
  between operations  0.65 us (1%)
    pallas_call x1, Pallas kernels, layer(): pl.pallas_call(layer_kernel, out_shape=OUT_SHAPES, in_specs=[HB] * 20, ou...  49.2 us
    pallas_call x1, Pallas kernels, shards(): pl.pallas_call(finish_kernel, out_shape=OUT_SHAPES, in_specs=[VM] * 3, ou...  1.39 us

profile of v3, /device:TPU:1, one launch (start us, length us, event | category | flops | bytes accessed | tf_op | source)
XLA Modules:
  0.0 51.3 jit_solution(16870536553615725745)
XLA Ops:
  0.6 49.2 %layer.1 = (bf16[8,2048]{1,0:T(8,128)(2,1)}, bf16[16,128]{1,0:T(8,128)(2,1)}, bf16[16,128]{1,0:T(8,128)(2,1)}) custom-call(bf16[2,8,2048]{2,1,0:T(8,128)(2,1)} %bitcast.14, f32[1,2048]{1,0:T(1,128)} %bitcast.15, f32[1,16]{1,0:T(1,128)} %bitcast.18, s32[16]{0:T(128)} %lengths_h.1, f32[1,2048]{1,0:T(1,128)} %bitcast.16, bf16[2048]{0:T(1024)(128)(2,1)} %mix_h.1, ...), custom_call_target="tpu_custom_call" | custom-call | tf_op jit(solution)/shard_map/layer/pallas_call | solution.py:572
  49.9 1.4 %finish.1 = (bf16[8,2048]{1,0:T(8,128)(2,1)}, bf16[16,128]{1,0:T(8,128)(2,1)}, bf16[16,128]{1,0:T(8,128)(2,1)}) custom-call(bf16[8,2048]{1,0:T(8,128)(2,1)} %get-tuple-element.6.a, bf16[16,128]{1,0:T(8,128)(2,1)} %get-tuple-element.7.b, bf16[16,128]{1,0:T(8,128)(2,1)} %get-tuple-element.8.c), custom_call_target="tpu_custom_call" | custom-call | tf_op jit(solution)/shard_map/finish/pallas_call | solution.py:637
